TPU v7x, 32 devices: a whole 2x2x4 slice. The times are simulated.
32 devices in a mesh: grp: 2 (over y), sp: 4 (over z), tp: 4 (over x, core).
Axes of the slice: x: 2, y: 2, z: 4, core: 2. Of those that a mesh axis runs over, the one named last changes fastest.
Arguments:
- tokens: bfloat16 [4096, 2048], P(('grp', 'sp')), parts along dimension 0, may hold values from -6 to 6
- fresh_token_input: bfloat16 [4096], P('grp'), parts along dimension 0, may hold values from -6 to 6
- value_matrix: bfloat16 [2048, 2048], P(None, 'tp'), may hold values from -0.125 to 0.125
- write_matrix: bfloat16 [2048, 1024], P(None, 'tp'), may hold values from -0.125 to 0.125
- read_matrix: bfloat16 [2048, 1024], P(None, 'tp'), may hold values from -0.125 to 0.125
- gate_matrix: bfloat16 [2048, 2048], P(None, 'tp'), may hold values from -0.125 to 0.125
- step_matrix: bfloat16 [2048, 32], replicated, may hold values from -0.125 to 0.125
- value_filter_taps: bfloat16 [4, 2048], replicated, may hold values from -3 to 3
- write_filter_taps: bfloat16 [4, 1024], replicated, may hold values from -3 to 3
- read_filter_taps: bfloat16 [4, 1024], replicated, may hold values from -3 to 3
- head_log_decay: float32 [32], replicated
- step_offset_bias: float32 [32], replicated, may hold values from -3.5 to -2.5
- decay_spike: float32 [4096, 32], P(('grp', 'sp'), 'tp'), parts along dimension 0, may hold values from -3 to 0, as said below
- bypass_scale: float32 [32], replicated, may hold values from 0.5 to 2
- group_norm_scale: float32 [2048], replicated, may hold values from 0.1 to 1.9
Outputs:
- prompt_out: bfloat16 [4096, 2048], P(('grp', 'sp'), 'tp'), parts along dimension 0
- state_cache: bfloat16 [256, 2048], P(('grp', 'sp'), 'tp'), parts along dimension 0
- step_out: bfloat16 [1024, 4], P(('grp', 'tp'), 'sp'), parts along dimension 0
There are 2 independent parts, one for each index of `grp`. A program takes and returns all parts, laid end to end along the dimension named above; an argument that names none is the same for every part. Nothing has to cross between parts.
Inputs may be any that keep to these rules, and one draw needn't show every extreme that they name: `decay_spike`: never positive.
All inputs are finite; a program needn't handle non-finite values.
Results may differ from a plain program's by a relative error of at most 0.023.
Values may be sent and summed in bfloat16 or wider, within the bound.
A program may use at most 64 MiB of HBM per device.

v0:
```python
import jax
import jax.numpy as jnp
from jax import lax
from jax.sharding import PartitionSpec as P

HEAD = 64
STATE = 128
CONV = 4
BLOCK = 128
epsilon = 1e-06


def passed_along(block, axis, distance):
    devices = range(lax.axis_size(axis))
    route = [(i - distance, i) for i in devices if i - distance in devices]
    return lax.ppermute(block, axis, route)


def from_root(value, axis, source):
    kept = jnp.where(lax.axis_index(axis) == source, value, 0).astype(value.dtype)
    return lax.psum(kept, axis)


def project(operand, weights):
    return jnp.dot(operand, weights, preferred_element_type=jnp.float32).astype(jnp.bfloat16)


def apply_taps(previous, current, tap_weights):
    joined = jnp.concatenate([previous, current], axis=0).astype(jnp.float32)
    length = current.shape[0]
    summed = jnp.zeros(current.shape, jnp.float32)
    for offset in range(CONV):
        summed = summed + tap_weights[offset].astype(jnp.float32) * joined[offset : offset + length]
    return summed


def group_norm(gated_rows, groups):
    shaped = gated_rows.reshape(gated_rows.shape[:-1] + (groups, -1))
    normed = shaped * lax.rsqrt(jnp.mean(shaped * shaped, axis=-1, keepdims=True) + epsilon)
    return normed.reshape(gated_rows.shape)


def read_new(cached, stored_portion, read_part, new_decay, step_now, value_now):
    states = cached.astype(jnp.float32).reshape((cached.shape[0],) + value_now.shape)
    updated = (
        new_decay[None, :, :, None] * states
        + step_now[None, :, :, None] * stored_portion.T[:, :, None, None] * value_now[None]
    )
    return jnp.einsum("gn,ngep->gep", read_part, updated, precision=lax.Precision.HIGHEST)


def on_device(
    tokens,
    fresh_token_input,
    value_matrix,
    write_matrix,
    read_matrix,
    gate_matrix,
    step_matrix,
    value_filter_taps,
    write_filter_taps,
    read_filter_taps,
    head_log_decay,
    step_offset_bias,
    decay_spike,
    bypass_scale,
    group_norm_scale,
):
    head_rank = lax.axis_index("tp")
    sequence_rank = lax.axis_index("sp")
    sequence_count = lax.axis_size("sp")
    channels = value_matrix.shape[1]
    head_count = channels // HEAD
    map_width = write_matrix.shape[1]
    group_count = map_width // STATE
    per_group = head_count // group_count
    row_count = tokens.shape[0]
    head_start = head_rank * head_count
    local_count = STATE // sequence_count
    own_step = lax.dynamic_slice_in_dim(step_matrix, head_start, head_count, 1)
    own_value_taps = lax.dynamic_slice_in_dim(value_filter_taps, head_rank * channels, channels, 1)
    own_write_taps = lax.dynamic_slice_in_dim(
        write_filter_taps, head_rank * map_width, map_width, 1
    )
    own_read_taps = lax.dynamic_slice_in_dim(read_filter_taps, head_rank * map_width, map_width, 1)
    head_decay_rates = jnp.exp(lax.dynamic_slice_in_dim(head_log_decay, head_start, head_count, 0))
    own_bias = lax.dynamic_slice_in_dim(step_offset_bias, head_start, head_count, 0)
    own_skip = lax.dynamic_slice_in_dim(bypass_scale, head_start, head_count, 0)
    own_gain = lax.dynamic_slice_in_dim(group_norm_scale, head_rank * channels, channels, 0)
    value_rows = project(tokens, value_matrix)
    write_rows = project(tokens, write_matrix)
    read_rows = project(tokens, read_matrix)
    gate_rows = project(tokens, gate_matrix)
    step_raw = jnp.dot(tokens, own_step, preferred_element_type=jnp.float32)
    edge = row_count - (CONV - 1)
    tail_rows = (value_rows[edge:], write_rows[edge:], read_rows[edge:])
    before = passed_along((tail_rows[0], tail_rows[1], tail_rows[2]), "sp", 1)
    ending = (
        from_root(tail_rows[0], "sp", sequence_count - 1),
        from_root(tail_rows[1], "sp", sequence_count - 1),
        from_root(tail_rows[2], "sp", sequence_count - 1),
    )
    values = jax.nn.silu(apply_taps(before[0], value_rows, own_value_taps)).astype(jnp.bfloat16)
    writes = jax.nn.silu(apply_taps(before[1], write_rows, own_write_taps)).astype(jnp.bfloat16)
    reads = jax.nn.silu(apply_taps(before[2], read_rows, own_read_taps)).astype(jnp.bfloat16)
    step_length = jax.nn.softplus(step_raw + own_bias)
    log_decay_value = decay_spike - step_length * head_decay_rates
    blocks = row_count // BLOCK
    block_values = values.reshape(blocks, BLOCK, group_count, per_group, HEAD)
    block_writes = writes.reshape(blocks, BLOCK, group_count, STATE)
    block_reads = reads.reshape(blocks, BLOCK, group_count, STATE)
    block_steps = step_length.reshape(blocks, BLOCK, group_count, per_group)
    cumulative = jnp.cumsum(log_decay_value.reshape(blocks, BLOCK, group_count, per_group), axis=1)
    block_end = cumulative[:, -1]
    scaled = (
        (jnp.exp(block_end[:, None] - cumulative) * block_steps)[..., None]
        * block_values.astype(jnp.float32)
    ).astype(jnp.bfloat16)
    block_states = jnp.einsum(
        "bsgn,bsgep->bngep", block_writes, scaled, preferred_element_type=jnp.float32
    )
    running = jnp.zeros((STATE, group_count, per_group, HEAD), jnp.float32)
    inside = []
    for block_index in range(blocks):
        inside.append(running)
        running = (
            jnp.exp(block_end[block_index])[None, :, :, None] * running + block_states[block_index]
        )
    local_states = jnp.stack(inside)
    shard_fading_factor = jnp.sum(block_end, axis=0)
    before_block = jnp.cumsum(block_end, axis=0) - block_end
    decay_table = lax.all_gather(shard_fading_factor[None], "sp", axis=0, tiled=True)
    inclusive = jnp.cumsum(decay_table, axis=0)
    exclusive = inclusive - decay_table
    total_decay = inclusive[-1]
    row_pieces = lax.all_to_all(running[None], "sp", split_axis=1, concat_axis=0, tiled=True)
    ranks = jnp.arange(sequence_count)
    below = (ranks[None, :] < ranks[:, None])[:, :, None, None]
    prefix_weight = jnp.exp(jnp.where(below, exclusive[:, None] - inclusive[None, :], -jnp.inf))
    prefix_rows = jnp.einsum(
        "jkge,kngep->jngep", prefix_weight, row_pieces, precision=lax.Precision.HIGHEST
    )
    final_weight = jnp.exp(total_decay[None] - inclusive)
    final_rows = jnp.einsum(
        "kge,kngep->ngep", final_weight, row_pieces, precision=lax.Precision.HIGHEST
    )
    earlier_state = lax.all_to_all(prefix_rows, "sp", split_axis=0, concat_axis=1, tiled=True)[0]
    scores = jnp.einsum(
        "blgn,bsgn->bgls", block_reads, block_writes, preferred_element_type=jnp.float32
    )
    cum_heads = jnp.transpose(cumulative, (0, 2, 3, 1))
    decay_gaps = cum_heads[..., :, None] - cum_heads[..., None, :]
    step_heads = jnp.transpose(block_steps, (0, 2, 3, 1))
    causal = jnp.tril(jnp.ones((BLOCK, BLOCK), bool))
    mixing = (
        scores[:, :, None]
        * jnp.exp(jnp.where(causal, decay_gaps, -jnp.inf))
        * step_heads[..., None, :]
    ).astype(jnp.bfloat16)
    inner_part = jnp.einsum(
        "bgels,bsgep->blgep", mixing, block_values, preferred_element_type=jnp.float32
    )
    entering = jnp.exp(before_block)[:, None, :, :, None] * earlier_state[None] + local_states
    carried_part = jnp.exp(cumulative)[..., None] * jnp.einsum(
        "blgn,bngep->blgep",
        block_reads.astype(jnp.float32),
        entering,
        precision=lax.Precision.HIGHEST,
    )
    mixed_rows = (inner_part + carried_part).reshape(row_count, head_count, HEAD) + own_skip[
        None, :, None
    ] * values.astype(jnp.float32).reshape(row_count, head_count, HEAD)
    gated_rows = mixed_rows.reshape(row_count, channels) * jax.nn.silu(
        gate_rows.astype(jnp.float32)
    )
    prompt_out = (group_norm(gated_rows, group_count) * own_gain).astype(jnp.bfloat16)
    new_row = fresh_token_input[None]
    new_value = project(new_row, value_matrix)
    new_write = project(new_row, write_matrix)
    new_read = project(new_row, read_matrix)
    new_gate = project(new_row, gate_matrix)
    new_step = jax.nn.softplus(
        jnp.dot(new_row, own_step, preferred_element_type=jnp.float32)[0] + own_bias
    )
    new_values = jax.nn.silu(apply_taps(ending[0], new_value, own_value_taps)).astype(jnp.bfloat16)
    latest_stores = jax.nn.silu(apply_taps(ending[1], new_write, own_write_taps)).astype(
        jnp.bfloat16
    )
    new_reads = jax.nn.silu(apply_taps(ending[2], new_read, own_read_taps)).astype(jnp.bfloat16)
    value_now = new_values.astype(jnp.float32).reshape(group_count, per_group, HEAD)
    write_now = latest_stores.astype(jnp.float32).reshape(group_count, STATE)
    read_now = new_reads.astype(jnp.float32).reshape(group_count, STATE)
    new_decay = jnp.exp(-new_step * head_decay_rates).reshape(group_count, per_group)
    step_now = new_step.reshape(group_count, per_group)
    row_start = sequence_rank * local_count
    cache_rows = final_rows.reshape(local_count, channels).astype(jnp.bfloat16)
    stored_portion = lax.dynamic_slice_in_dim(write_now, row_start, local_count, 1)
    read_part = lax.dynamic_slice_in_dim(read_now, row_start, local_count, 1)
    partial_value = read_new(cache_rows, stored_portion, read_part, new_decay, step_now, value_now)
    reading = lax.psum(partial_value, "sp")
    new_mixed = reading + own_skip.reshape(group_count, per_group)[:, :, None] * value_now
    new_gated = new_mixed.reshape(1, channels) * jax.nn.silu(new_gate.astype(jnp.float32))
    step_whole = (group_norm(new_gated, group_count) * own_gain).astype(jnp.bfloat16)[0]
    step_table = step_whole.reshape(channels // sequence_count, sequence_count)
    step_out = lax.dynamic_slice_in_dim(step_table, sequence_rank, 1, 1)
    return (prompt_out, cache_rows, step_out)


def solution(mesh):
    placed = (
        P(("grp", "sp"), None),
        P("grp"),
        P(None, "tp"),
        P(None, "tp"),
        P(None, "tp"),
        P(None, "tp"),
        P(),
        P(),
        P(),
        P(),
        P(),
        P(),
        P(("grp", "sp"), "tp"),
        P(),
        P(),
    )
    return jax.shard_map(
        on_device,
        mesh=mesh,
        in_specs=placed,
        out_specs=(P(("grp", "sp"), "tp"), P(("grp", "sp"), "tp"), P(("grp", "tp"), "sp")),
        check_vma=False,
    )
```

profile of v0, /device:TPU:0, one launch (start us, length us, event | category | flops | bytes accessed | tf_op | source)
XLA Modules:
  0.0 126.4 jit_solution(4960432107386798171)
XLA Ops:
  0.7 1.6 %copy-done = bf16[512,2048]{1,0:T(8,128)(2,1)S(1)} copy-done((bf16[512,2048]{1,0:T(8,128)(2,1)S(1)}, bf16[512,2048]{1,0:T(8,128)(2,1)}, u32[]{:S(2)}) %copy-start) | copy-done | bytes 2097176
  2.2 1.9 %convolution_convert_fusion.2 = bf16[512,256]{1,0:T(8,128)(2,1)S(1)} fusion(bf16[512,2048]{1,0:T(8,128)(2,1)S(1)} %copy-done, bf16[2048,256]{1,0:T(8,128)(2,1)} %param.18), kind=kOutput, calls=%fused_computation.11 | convolution fusion | flops 537001984 | bytes 3407872 | tf_op jit(solution)/shard_map/dot_general | solution.py:25
  4.2 0.6 broadcast_select_fusion.1
  4.7 5.7 %collective-permute-start.2 = (bf16[3,256]{1,0:T(4,128)(2,1)}, bf16[3,256]{1,0:T(4,128)(2,1)}, u32[]{:S(2)}, u32[]{:S(2)}) collective-permute-start(bf16[3,256]{1,0:T(4,128)(2,1)} %get-tuple-element.57), channel_id=1, source_target_pairs={{0,4},{4,8},{8,12},{1,5},{5,9},{9,13},{2,6},{6,10},{10,14},{3,7},{... | collective-permute-start | bytes 4616 | tf_op jit(solution)/shard_map/ppermute | solution.py:16
  10.4 0.7 convolution_convert_fusion.3
  11.1 0.6 fusion.92
  11.8 3.6 %collective-permute-start.1 = (bf16[3,256]{1,0:T(4,128)(2,1)}, bf16[3,256]{1,0:T(4,128)(2,1)}, u32[]{:S(2)}, u32[]{:S(2)}) collective-permute-start(bf16[3,256]{1,0:T(4,128)(2,1)} %get-tuple-element.54), channel_id=1, source_target_pairs={{0,4},{4,8},{8,12},{1,5},{5,9},{9,13},{2,6},{6,10},{10,14},{3,7},{... | collective-permute-start | bytes 4616 | tf_op jit(solution)/shard_map/ppermute | solution.py:16
  15.4 1.3 convolution_convert_fusion.1
  16.7 0.8 copy-done.8
  17.5 0.6 fusion.91
  18.1 3.5 %collective-permute-start = (bf16[3,512]{1,0:T(4,128)(2,1)}, bf16[3,512]{1,0:T(4,128)(2,1)}, u32[]{:S(2)}, u32[]{:S(2)}) collective-permute-start(bf16[3,512]{1,0:T(4,128)(2,1)} %get-tuple-element.52), channel_id=1, source_target_pairs={{0,4},{4,8},{8,12},{1,5},{5,9},{9,13},{2,6},{6,10},{10,14},{3,7},{... | collective-permute-start | bytes 9224 | tf_op jit(solution)/shard_map/ppermute | solution.py:16
  21.6 0.5 iota_compare_fusion.1
  22.4 1.5 %fusion.96 = f32[1,256]{1,0:T(1,128)S(1)} fusion(bf16[2048,1]{0,1:T(2,128)(2,1)S(1)} %reshape.251, bf16[2048,256]{1,0:T(8,128)(2,1)} %param.19), kind=kOutput, calls=%fused_computation.194 | convolution fusion | flops 1048576 | bytes 1053696 | tf_op jit(solution)/shard_map/dot_general | solution.py:25
  24.5 0.7 multiply_exponential_fusion
  25.1 0.7 multiply_subtract_fusion
  26.3 0.6 fusion.76
  27.1 2.0 %fusion.99 = f32[1,512]{1,0:T(1,128)S(1)} fusion(bf16[2048,1]{0,1:T(2,128)(2,1)S(1)} %reshape.251, bf16[2048,512]{1,0:T(8,128)(2,1)} %param.20), kind=kOutput, calls=%fused_computation.197 | convolution fusion | flops 2097152 | bytes 2103296 | tf_op jit(solution)/shard_map/dot_general | solution.py:25
  29.1 7.6 %all-gather.1 = f32[4,2,4]{2,1,0:T(2,128)S(1)} all-gather(f32[1,2,4]{2,1,0:T(2,128)S(1)} %bitcast.152), channel_id=2, replica_groups=mesh['grp'=2,'sp'=4,'tp'=4] {'sp'}, dimensions={0}, use_global_device_ids=true | all-gather | bytes 160 | tf_op jit(solution)/shard_map/all_gather | solution.py:132
  36.7 10.5 %all-reduce = (bf16[3,512]{1,0:T(4,128)(2,1)S(1)}, bf16[3,256]{1,0:T(4,128)(2,1)S(1)}, bf16[3,256]{1,0:T(4,128)(2,1)S(1)}) all-reduce(bf16[3,512]{1,0:T(4,128)(2,1)S(1)} %get-tuple-element.53, bf16[3,256]{1,0:T(4,128)(2,1)S(1)} %get-tuple-element.56, ...), channel_id=1, replica_groups=mesh['grp'=2,'sp'=4,'tp'=4] {'sp'}, use_global_device_ids=true, to_apply=%region_7.8 | all-reduce | flops 3072 | bytes 12288 | tf_op jit(solution)/shard_map/psum | solution.py:21
  47.3 0.7 convert_convert_fusion
  48.1 1.0 copy.149
  49.2 0.7 convert_reduce_fusion.1
  49.9 2.4 %fusion.90 = (f32[4,128,2,4]{3,2,1,0:T(2,128)}, f32[4,128,2,4]{3,2,1,0:T(2,128)S(1)}) fusion(f32[4,128,2,4]{3,2,1,0:T(2,128)S(1)} %fusion.94, f32[4,128,2,4]{3,2,1,0:T(2,128)} %copy.149, f32[4,2,4]{2,1,0:T(2,128)S(1)} %get-tuple-element.47), kind=kLoop, calls=%fused_computation.187 | loop fusion | flops 8192 | bytes 65664 | tf_op jit(solution)/shard_map/exp | solution.py:164
  52.4 0.7 convert_reduce_fusion
  53.0 0.6 fusion.81
  53.7 0.7 dynamic_slice.39
  54.5 0.7 mul.552
  55.2 0.7 mul.510
  55.9 1.3 %mul.529 = f32[2,4]{1,0:T(2,128)} reshape(f32[8]{0:T(128)} %get-tuple-element.28) | data formatting | bytes 64 | tf_op jit(solution)/shard_map/mul | solution.py:46
  57.6 1.3 %copy.148 = f32[4,128,2,4]{1,3,2,0:T(4,128)S(1)} copy(f32[4,128,2,4]{3,2,1,0:T(2,128)} %get-tuple-element.44) | data formatting | bytes 32768 | tf_op jit(solution)/shard_map/exp | solution.py:164
  59.1 0.6 pad.6.clone
  59.7 0.7 maximum_convert_fusion.2
  60.5 1.0 multiply_convert_fusion.5
  61.5 0.8 maximum_convert_fusion.1
  62.8 0.8 maximum_convert_fusion
  63.6 1.3 %multiply_convert_fusion.4 = bf16[512,512]{1,0:T(8,128)(2,1)S(1)} fusion(f32[515,512]{1,0:T(8,128)S(1)} %maximum_convert_fusion, f32[512]{0:T(512)} %bitcast.141, f32[512]{0:T(512)} %bitcast.140, f32[512]{0:T(512)S(1)} %bitcast.139, f32[512]{0:T(512)S(1)} %bitcast.138), kind=kLoop, calls=%fused_computation.44 | loop fusion | flops 3145728 | bytes 4726784 | tf_op jit(solution)/shard_map/convert_element_type | solution.py:103
  65.0 1.0 copy.140
  66.0 2.0 %reshape.229 = bf16[4,128,2,4,64]{1,0,4,3,2:T(4,128)(2,1)} reshape(bf16[512,512]{0,1:T(8,128)(2,1)} %copy.140) | data formatting | bytes 1048576 | tf_op jit(solution)/shard_map/reshape | solution.py:109
  68.0 1.3 multiply_convert_fusion.3
  69.5 1.0 slice_add_fusion
  70.8 1.2 reshape.274
  72.0 3.6 %all-to-all-start = ((f32[4,1,16384]{2,1,0:T(1,128)}), f32[4,1,16384]{2,1,0:T(1,128)S(1)}, u32[]{:S(2)}, u32[]{:S(2)}) async-start(f32[4,1,16384]{2,1,0:T(1,128)} %reshape.274), calls=%async_computation | async-start | bytes 524288 | tf_op jit(solution)/shard_map/all_to_all | solution.py:136
  75.9 3.0 %convolution_bitcast_fusion.2 = f32[4,128,2,4,64]{1,4,3,2,0:T(8,128)} fusion(f32[4,2,4,128]{3,2,1,0:T(4,128)S(1)} %copy.146, f32[4,2,4,128]{3,2,1,0:T(4,128)S(1)} %copy.144, f32[4,2,128,128]{3,2,1,0:T(8,128)S(1)} %fusion.40, pred[128,128]{1,0:T(8,128)(4,1)S(1)} %iota_compare_fusion, bf16[4,128,2,4,64]{1,0,4,3,2:T(4,128)(2,1)} %reshape.229), kind=kOutput, calls=%fused_computation.5 | convolution fusion | flops 69730304 | bytes 2146304 | tf_op jit(solution)/shard_map/bgels,bsgep->blgep/dot_general | solution.py:160
  78.8 3.3 %all-to-all-done = f32[4,1,16384]{2,1,0:T(1,128)S(1)} async-done(((f32[4,1,16384]{2,1,0:T(1,128)}), f32[4,1,16384]{2,1,0:T(1,128)S(1)}, u32[]{:S(2)}, u32[]{:S(2)}) %all-to-all-start) | async-done | bytes 262176 | tf_op jit(solution)/shard_map/all_to_all | solution.py:136
  82.1 0.5 broadcast.118
  82.7 1.3 %reduce.9 = f32[4,16384]{1,0:T(4,128)S(1)} reduce(f32[4,1,16384]{2,1,0:T(1,128)S(1)} %all-to-all-done, f32[]{:T(128)} %broadcast.118), dimensions={1}, to_apply=%all_to_all.6.reduce_sub_computation | reduce | bytes 524292 | tf_op jit(solution)/shard_map/all_to_all | solution.py:136
  84.4 1.3 %fusion.35 = bf16[2,4,1,32,64]{4,2,3,1,0:T(2,128)(2,1)S(1)} fusion(f32[4,2,4,1,1]{0,3,4,2,1:T(1,128)S(1)} %copy.173, f32[4,32,2,4,64]{4,3,2,1,0:T(4,128)S(1)} %bitcast.123), kind=kOutput, calls=%fused_computation.69 | convolution fusion | flops 786432 | bytes 295040 | tf_op jit(solution)/shard_map/kge,kngep->ngep/dot_general | solution.py:144
  85.7 1.3 %convolution_bitcast_fusion.3 = f32[4,32,2,4,64]{4,0,1,3,2:T(4,128)S(1)} fusion(f32[4,32,2,4,64]{4,3,2,1,0:T(4,128)S(1)} %bitcast.124, f32[4,2,4]{0,2,1:T(4,128)S(1)} %copy.156, f32[4,2,4]{0,2,1:T(4,128)S(1)} %copy.155, pred[4,4]{1,0:T(4,128)(4,1)S(1)} %copy-done.30), kind=kOutput, calls=%fused_computation.10 | convolution fusion | flops 3145984 | bytes 524560 | tf_op jit(solution)/shard_map/jkge,kngep->jngep/dot_general | solution.py:140
  87.1 1.0 reshape.276
  88.1 3.4 %all-to-all-start.1 = ((f32[4,1,16384]{2,1,0:T(1,128)}), f32[4,1,16384]{2,1,0:T(1,128)S(1)}, u32[]{:S(2)}, u32[]{:S(2)}) async-start(f32[4,1,16384]{2,1,0:T(1,128)} %reshape.276), calls=%async_computation.1 | async-start | bytes 524288 | tf_op jit(solution)/shard_map/all_to_all | solution.py:147
  91.9 12.2 %psum.31 = f32[2,4,64]{2,1,0:T(4,128)S(1)} all-reduce(f32[2,4,64]{2,1,0:T(4,128)S(1)} %bitcast.137), channel_id=1, replica_groups=mesh['grp'=2,'sp'=4,'tp'=4] {'sp'}, use_global_device_ids=true, to_apply=%region_8.9 | all-reduce | flops 512 | bytes 4096 | tf_op jit(solution)/shard_map/psum | solution.py:200
  104.5 0.7 convert_element_type.211
  105.3 0.8 multiply_convert_fusion.7
  106.3 0.6 copy.168
  106.9 1.3 %reduce.10 = f32[4,16384]{1,0:T(4,128)S(1)} reduce(f32[4,1,16384]{2,1,0:T(1,128)S(1)} %all-to-all-done.1, f32[]{:T(128)} %broadcast.118), dimensions={1}, to_apply=%all_to_all.8.reduce_sub_computation | reduce | bytes 524292 | tf_op jit(solution)/shard_map/all_to_all | solution.py:147
  108.5 0.9 copy.160
  109.4 2.3 %fusion.1 = f32[4,128,2,4,64]{1,4,3,2,0:T(8,128)S(1)} fusion(f32[4,128,2,4,64]{1,4,3,2,0:T(8,128)} %convolution_bitcast_fusion.2, f32[1,128,2,4,64]{1,4,3,2,0:T(8,128)} %get-tuple-element.41, f32[1,128,2,4,64]{1,4,3,2,0:T(8,128)} %get-tuple-element.42, f32[1,128,2,4,64]{1,4,3,2,0:T(8,128)} %get-tuple-element.43, f32[4]{0:T(128)S(1)} %copy-done.31, ...), kind=kOutput, calls=%fused_computation.4 | convolution fusion | flops 404488192 | bytes 3424400 | tf_op jit(solution)/shard_map/blgn,bngep->blgep/dot_general | solution.py:164
  111.7 1.8 %copy.184 = f32[4,128,2,4,64]{4,3,2,1,0:T(4,128)} copy(f32[4,128,2,4,64]{1,4,3,2,0:T(8,128)S(1)} %fusion.1) | data formatting | bytes 2097152 | tf_op jit(solution)/shard_map/reshape | solution.py:170
  113.5 3.5 %reshape.263 = f32[512,512]{1,0:T(8,128)} reshape(f32[4,128,2,4,64]{4,3,2,1,0:T(4,128)} %copy.184) | data formatting | bytes 2097152 | tf_op jit(solution)/shard_map/reshape | solution.py:170
  117.0 4.6 %fusion.93 = (f32[512,512]{1,0:T(8,128)}, f32[512,512]{1,0:T(8,128)}) fusion(bf16[512,2048]{1,0:T(8,128)(2,1)S(1)} %copy-done, bf16[2048,512]{1,0:T(8,128)(2,1)} %param.20, f32[512,512]{1,0:T(8,128)} %reshape.263, bf16[512,512]{1,0:T(8,128)(2,1)S(1)} %copy-done.2, f32[512]{0:T(512)S(1)} %copy-done.25), kind=kOutput, calls=%fused_computation.190 | convolution fusion | flops 1076625408 | bytes 7866368 | tf_op jit(solution)/shard_map/dot_general | solution.py:25
  121.7 1.9 %mul.516 = f32[512,2,256]{2,1,0:T(2,128)S(1)} reshape(f32[512,512]{1,0:T(8,128)} %get-tuple-element.63) | data formatting | bytes 2097152 | tf_op jit(solution)/shard_map/mul | solution.py:39
  123.5 0.6 reduce_sum.28
  124.2 0.6 mul.517
  125.4 1.1 multiply_convert_fusion.2
  (128 shorter events, 6.4 us)
Async XLA Ops:
  0.6 1.6 %copy-start = (bf16[512,2048]{1,0:T(8,128)(2,1)S(1)}, bf16[512,2048]{1,0:T(8,128)(2,1)}, u32[]{:S(2)}) copy-start(bf16[512,2048]{1,0:T(8,128)(2,1)} %param.15) | copy-start | bytes 6291460
  0.6 9.8 %copy-start.6 = (bf16[2048,256]{1,0:T(8,128)(2,1)S(1)}, bf16[2048,256]{1,0:T(8,128)(2,1)}, u32[]{:S(2)}) copy-start(bf16[2048,256]{1,0:T(8,128)(2,1)} %param.19) | copy-start | bytes 3145732
  4.2 11.3 %copy-start.3 = (bf16[2048,512]{1,0:T(8,128)(2,1)S(1)}, bf16[2048,512]{1,0:T(8,128)(2,1)}, u32[]{:S(2)}) copy-start(bf16[2048,512]{1,0:T(8,128)(2,1)} %param.17) | copy-start | bytes 6291460
  4.7 55.0 %collective-permute-start.2 = (bf16[3,256]{1,0:T(4,128)(2,1)}, bf16[3,256]{1,0:T(4,128)(2,1)}, u32[]{:S(2)}, u32[]{:S(2)}) collective-permute-start(bf16[3,256]{1,0:T(4,128)(2,1)} %get-tuple-element.57), channel_id=1, source_target_pairs={{0,4},{4,8},{8,12},{1,5},{5,9},{9,13},{2,6},{6,10},{10,14},{3,7},{... | collective-permute-start | bytes 4616 | tf_op jit(solution)/shard_map/ppermute | solution.py:16
  11.1 0.7 copy-start.10
  11.8 10.3 %copy-start.23 = (bf16[2048]{0:T(1024)(128)(2,1)S(1)}, bf16[2048]{0:T(1024)(128)(2,1)}, u32[]{:S(2)}) copy-start(bf16[2048]{0:T(1024)(128)(2,1)} %param.16) | copy-start | bytes 12292
  11.8 10.3 %copy-start.5 = (bf16[2048,256]{1,0:T(8,128)(2,1)S(1)}, bf16[2048,256]{1,0:T(8,128)(2,1)}, u32[]{:S(2)}) copy-start(bf16[2048,256]{1,0:T(8,128)(2,1)} %param.18) | copy-start | bytes 3145732
  11.8 49.6 %collective-permute-start.1 = (bf16[3,256]{1,0:T(4,128)(2,1)}, bf16[3,256]{1,0:T(4,128)(2,1)}, u32[]{:S(2)}, u32[]{:S(2)}) collective-permute-start(bf16[3,256]{1,0:T(4,128)(2,1)} %get-tuple-element.54), channel_id=1, source_target_pairs={{0,4},{4,8},{8,12},{1,5},{5,9},{9,13},{2,6},{6,10},{10,14},{3,7},{... | collective-permute-start | bytes 4616 | tf_op jit(solution)/shard_map/ppermute | solution.py:16
  16.7 0.8 copy-start.8
  18.1 44.7 %collective-permute-start = (bf16[3,512]{1,0:T(4,128)(2,1)}, bf16[3,512]{1,0:T(4,128)(2,1)}, u32[]{:S(2)}, u32[]{:S(2)}) collective-permute-start(bf16[3,512]{1,0:T(4,128)(2,1)} %get-tuple-element.52), channel_id=1, source_target_pairs={{0,4},{4,8},{8,12},{1,5},{5,9},{9,13},{2,6},{6,10},{10,14},{3,7},{... | collective-permute-start | bytes 9224 | tf_op jit(solution)/shard_map/ppermute | solution.py:16
  21.6 2.3 %copy-start.4 = (bf16[2048,512]{1,0:T(8,128)(2,1)S(1)}, bf16[2048,512]{1,0:T(8,128)(2,1)}, u32[]{:S(2)}) copy-start(bf16[2048,512]{1,0:T(8,128)(2,1)} %param.17) | copy-start | bytes 6291460
  22.1 2.2 %copy-start.33 = (f32[32]{0:T(128)S(1)}, f32[32]{0:T(128)}, u32[]{:S(2)}) copy-start(f32[32]{0:T(128)} %param.26) | copy-start | bytes 388
  22.2 2.3 %copy-start.32 = (f32[32]{0:T(128)S(1)}, f32[32]{0:T(128)}, u32[]{:S(2)}) copy-start(f32[32]{0:T(128)} %param.25) | copy-start | bytes 388
  22.2 3.0 %copy-start.12 = (f32[512,8]{0,1:T(8,128)S(1)}, f32[512,8]{0,1:T(8,128)}, u32[]{:S(2)}) copy-start(f32[512,8]{0,1:T(8,128)} %param.27) | copy-start | bytes 49156
  22.4 2.0 %copy-start.13 = (bf16[2048,32]{0,1:T(8,128)(2,1)S(1)}, bf16[2048,32]{0,1:T(8,128)(2,1)}, u32[]{:S(2)}) copy-start(bf16[2048,32]{0,1:T(8,128)(2,1)} %param.21) | copy-start | bytes 393220
  25.8 21.5 %copy-start.26 = (bf16[4,1024]{1,0:T(4,128)(2,1)S(1)}, bf16[4,1024]{1,0:T(4,128)(2,1)}, u32[]{:S(2)}) copy-start(bf16[4,1024]{1,0:T(4,128)(2,1)} %param.23) | copy-start | bytes 24580
  26.1 23.0 %copy-start.27 = (bf16[4,1024]{1,0:T(4,128)(2,1)S(1)}, bf16[4,1024]{1,0:T(4,128)(2,1)}, u32[]{:S(2)}) copy-start(bf16[4,1024]{1,0:T(4,128)(2,1)} %param.24) | copy-start | bytes 24580
  27.1 25.3 %copy-start.22 = (bf16[4,2048]{1,0:T(4,128)(2,1)S(1)}, bf16[4,2048]{1,0:T(4,128)(2,1)}, u32[]{:S(2)}) copy-start(bf16[4,2048]{1,0:T(4,128)(2,1)} %param.22) | copy-start | bytes 49156
  57.6 3.9 %copy-start.11 = (bf16[512,256]{1,0:T(8,128)(2,1)S(1)}, bf16[512,256]{1,0:T(8,128)(2,1)}, u32[]{:S(2)}) copy-start(bf16[512,256]{1,0:T(8,128)(2,1)} %copy-done.10) | copy-start | bytes 786436
  59.1 3.1 %copy-start.18 = (f32[1,256]{1,0:T(1,128)S(1)}, f32[1,256]{1,0:T(1,128)}, u32[]{:S(2)}) copy-start(f32[1,256]{1,0:T(1,128)} %get-tuple-element.24) | copy-start | bytes 3076
  59.1 3.2 %copy-start.19 = (f32[1,256]{1,0:T(1,128)S(1)}, f32[1,256]{1,0:T(1,128)}, u32[]{:S(2)}) copy-start(f32[1,256]{1,0:T(1,128)} %get-tuple-element.25) | copy-start | bytes 3076
  59.1 3.2 %copy-start.20 = (f32[1,256]{1,0:T(1,128)S(1)}, f32[1,256]{1,0:T(1,128)}, u32[]{:S(2)}) copy-start(f32[1,256]{1,0:T(1,128)} %get-tuple-element.26) | copy-start | bytes 3076
  59.1 3.2 %copy-start.21 = (f32[1,256]{1,0:T(1,128)S(1)}, f32[1,256]{1,0:T(1,128)}, u32[]{:S(2)}) copy-start(f32[1,256]{1,0:T(1,128)} %get-tuple-element.27) | copy-start | bytes 3076
  61.5 1.3 %copy-start.9 = (bf16[512,512]{1,0:T(8,128)(2,1)S(1)}, bf16[512,512]{1,0:T(8,128)(2,1)}, u32[]{:S(2)}) copy-start(bf16[512,512]{1,0:T(8,128)(2,1)} %copy-done.8) | copy-start | bytes 1572868
  65.0 4.5 %copy-start.1 = (bf16[512,512]{1,0:T(8,128)(2,1)}, bf16[512,512]{1,0:T(8,128)(2,1)S(1)}, u32[]{:S(2)}) copy-start(bf16[512,512]{1,0:T(8,128)(2,1)S(1)} %multiply_convert_fusion.4) | copy-start | bytes 1572868
  66.0 3.5 %copy-start.14 = (f32[2,4]{1,0:T(2,128)S(1)}, f32[2,4]{1,0:T(2,128)}, u32[]{:S(2)}) copy-start(f32[2,4]{1,0:T(2,128)} %get-tuple-element.48) | copy-start | bytes 100
  66.0 3.5 %copy-start.15 = (f32[2,4]{1,0:T(2,128)S(1)}, f32[2,4]{1,0:T(2,128)}, u32[]{:S(2)}) copy-start(f32[2,4]{1,0:T(2,128)} %get-tuple-element.49) | copy-start | bytes 100
  68.0 1.6 %copy-start.16 = (f32[2,4]{1,0:T(2,128)S(1)}, f32[2,4]{1,0:T(2,128)}, u32[]{:S(2)}) copy-start(f32[2,4]{1,0:T(2,128)} %get-tuple-element.50) | copy-start | bytes 100
  68.0 1.6 %copy-start.17 = (f32[2,4]{1,0:T(2,128)S(1)}, f32[2,4]{1,0:T(2,128)}, u32[]{:S(2)}) copy-start(f32[2,4]{1,0:T(2,128)} %get-tuple-element.51) | copy-start | bytes 100
  72.0 10.2 %all-to-all-start = ((f32[4,1,16384]{2,1,0:T(1,128)}), f32[4,1,16384]{2,1,0:T(1,128)S(1)}, u32[]{:S(2)}, u32[]{:S(2)}) async-start(f32[4,1,16384]{2,1,0:T(1,128)} %reshape.274), calls=%async_computation | async-start | bytes 524288 | tf_op jit(solution)/shard_map/all_to_all | solution.py:136
  75.9 9.8 %copy-start.30 = (pred[4,4]{1,0:T(4,128)(4,1)S(1)}, pred[4,4]{1,0:T(4,128)(4,1)}, u32[]{:S(2)}) copy-start(pred[4,4]{1,0:T(4,128)(4,1)} %iota_compare_fusion.1) | copy-start | bytes 52
  84.3 7.2 %copy-start.28 = (f32[2,4]{1,0:T(2,128)S(1)}, f32[2,4]{1,0:T(2,128)}, u32[]{:S(2)}) copy-start(f32[2,4]{1,0:T(2,128)} %mul.529) | copy-start | bytes 100
  84.3 7.4 %copy-start.24 = (bf16[2,32,1,1]{1,0,2,3:T(2,128)(2,1)S(1)}, bf16[2,32,1,1]{1,0,2,3:T(2,128)(2,1)}, u32[]{:S(2)}) copy-start(bf16[2,32,1,1]{1,0,2,3:T(2,128)(2,1)} %fusion.81) | copy-start | bytes 388
  85.7 18.4 %copy-start.29 = (f32[2,4]{1,0:T(2,128)S(1)}, f32[2,4]{1,0:T(2,128)}, u32[]{:S(2)}) copy-start(f32[2,4]{1,0:T(2,128)} %mul.552) | copy-start | bytes 100
  88.1 18.8 %all-to-all-start.1 = ((f32[4,1,16384]{2,1,0:T(1,128)}), f32[4,1,16384]{2,1,0:T(1,128)S(1)}, u32[]{:S(2)}, u32[]{:S(2)}) async-start(f32[4,1,16384]{2,1,0:T(1,128)} %reshape.276), calls=%async_computation.1 | async-start | bytes 524288 | tf_op jit(solution)/shard_map/all_to_all | solution.py:147
  91.5 17.9 %copy-start.31 = (f32[4]{0:T(128)S(1)}, f32[4]{0:T(128)}, u32[]{:S(2)}) copy-start(f32[4]{0:T(128)} %pad.6.clone) | copy-start | bytes 52
  113.5 3.5 %copy-start.2 = (bf16[512,512]{1,0:T(8,128)(2,1)S(1)}, bf16[512,512]{1,0:T(8,128)(2,1)}, u32[]{:S(2)}) copy-start(bf16[512,512]{1,0:T(8,128)(2,1)} %copy-done.1) | copy-start | bytes 1572868
  113.5 3.5 %copy-start.25 = (f32[512]{0:T(512)S(1)}, f32[512]{0:T(512)}, u32[]{:S(2)}) copy-start(f32[512]{0:T(512)} %mul.510) | copy-start | bytes 6148
  124.2 1.2 copy-start.7
where the time goes:
time: 127 us; the launch traced here: 126 us
  blocking collectives  30.3 us (24%)
  local copies, waits for them, and re-layouts  28.8 us (23%)
  matrix products  22.6 us (18%)
  other arithmetic  20.4 us (16%)
  starting transfers between devices  19.8 us (16%)
  waiting for transfers between devices  3.3 us (3%)
    ppermute x3, starting transfers between devices, passed_along(): return lax.ppermute(block, axis, route)  12.8 us
    dot_general x8, matrix products, project(): jnp.dot(operand, weights, preferred_element_type=jnp.float32)  12.6 us
    psum x1, blocking collectives, on_device(): reading = lax.psum(partial_value, 'sp')  12.2 us
    psum x1, blocking collectives, from_root(): return lax.psum(kept, axis)  10.5 us
    all_gather x1, blocking collectives, on_device(): lax.all_gather(shard_fading_factor[None], 'sp', axis=0, tiled=True)  7.58 us
    unnamed x75, local copies, waits for them, and re-layouts  6.63 us
    reshape x2, local copies, waits for them, and re-layouts, on_device(): (inner_part + carried_part).reshape(row_count, head_count, HEAD)  5.28 us
    all_to_all x1, starting transfers between devices, on_device(): lax.all_to_all(running[None], 'sp', split_axis=1, concat_axis=0, tiled=True)  3.58 us
  transfers between devices with their start and end apart: 5, of which 1 were waited for; matrix products, arithmetic and copies ran while one was open for 26% of the time, Pallas kernels for 0%

commit v1 on v0

--- a/solution.py
+++ b/solution.py
@@ -129,7 +129,9 @@
     local_states = jnp.stack(inside)
     shard_fading_factor = jnp.sum(block_end, axis=0)
     before_block = jnp.cumsum(block_end, axis=0) - block_end
-    decay_table = lax.all_gather(shard_fading_factor[None], "sp", axis=0, tiled=True)
+    local_x = shard_fading_factor[None]
+    frame_out = jax.lax.all_to_all(jnp.stack(jax.lax.axis_size("sp") * [local_x]), "sp", 0, 0)
+    decay_table = jnp.concatenate(frame_out, axis=0)
     inclusive = jnp.cumsum(decay_table, axis=0)
     exclusive = inclusive - decay_table
     total_decay = inclusive[-1]

time: 127 us -> 137 us (1.079)
  blocking collectives: 30.3 us -> 22.2 us
  matrix products: 22.6 us -> 29.1 us
  other arithmetic: 20.4 us -> 24.6 us
  local copies, waits for them, and re-layouts: 28.8 us -> 32.2 us
  starting transfers between devices: 19.8 us -> 23.1 us
    all_gather x1 -> x0, blocking collectives: 7.58 us -> none  [on_device(): lax.all_gather(shard_fading_factor[None], 'sp', axis=0, tiled=True)]
    dot_general x8, matrix products: 12.6 us -> 16.1 us  [project(): jnp.dot(operand, weights, preferred_element_type=jnp.float32)]
    all_to_all x0 -> x1, starting transfers between devices: none -> 3.23 us  [on_device(): jax.lax.all_to_all(jnp.stack(jax.lax.axis_size('sp') * [local_x]), 'sp',...]
    unnamed x75 -> x45, local copies, waits for them, and re-layouts: 6.63 us -> 6.51 us
  transfers between devices with their start and end apart: 5 -> 6, of which waited for: 1 -> 1; matrix products, arithmetic and copies ran while one was open for 26% -> 33% of each run, Pallas kernels for 0% -> 0%
where the time goes in v1:
time: 137 us; the launch traced here: 136 us
  local copies, waits for them, and re-layouts  32.2 us (24%)
  matrix products  29.1 us (21%)
  other arithmetic  24.6 us (18%)
  starting transfers between devices  23.1 us (17%)
  blocking collectives  22.2 us (16%)
  waiting for transfers between devices  3.35 us (2%)
    dot_general x8, matrix products, project(): jnp.dot(operand, weights, preferred_element_type=jnp.float32)  16.1 us
    ppermute x3, starting transfers between devices, passed_along(): return lax.ppermute(block, axis, route)  12.9 us
    psum x1, blocking collectives, on_device(): reading = lax.psum(partial_value, 'sp')  12.2 us
    psum x1, blocking collectives, from_root(): return lax.psum(kept, axis)  9.99 us
    unnamed x45, local copies, waits for them, and re-layouts  6.51 us
    reshape x2, local copies, waits for them, and re-layouts, on_device(): (inner_part + carried_part).reshape(row_count, head_count, HEAD)  5.33 us
    convert_element_type x5, other arithmetic, apply_taps(): joined = jnp.concatenate([previous, current], axis=0).astype(jnp.float32)  3.62 us
    all_to_all x1, starting transfers between devices, on_device(): lax.all_to_all(running[None], 'sp', split_axis=1, concat_axis=0, tiled=True)  3.58 us
  transfers between devices with their start and end apart: 6, of which 1 were waited for; matrix products, arithmetic and copies ran while one was open for 33% of the time, Pallas kernels for 0%

profile of v1, /device:TPU:0, one launch (start us, length us, event | category | flops | bytes accessed | tf_op | source)
XLA Modules:
  0.0 135.7 jit_solution(11693514717989658256)
XLA Ops:
  0.7 1.6 %copy-done = bf16[512,2048]{1,0:T(8,128)(2,1)S(1)} copy-done((bf16[512,2048]{1,0:T(8,128)(2,1)S(1)}, bf16[512,2048]{1,0:T(8,128)(2,1)}, u32[]{:S(2)}) %copy-start) | copy-done | bytes 2097176
  2.2 1.9 %convolution_convert_fusion.2 = bf16[512,256]{1,0:T(8,128)(2,1)S(1)} fusion(bf16[512,2048]{1,0:T(8,128)(2,1)S(1)} %copy-done, bf16[2048,256]{1,0:T(8,128)(2,1)} %param.18), kind=kOutput, calls=%fused_computation.11 | convolution fusion | flops 537001984 | bytes 3407872 | tf_op jit(solution)/shard_map/dot_general | solution.py:25
  4.8 5.5 %collective-permute-start.2 = (bf16[3,256]{1,0:T(4,128)(2,1)}, bf16[3,256]{1,0:T(4,128)(2,1)}, u32[]{:S(2)}, u32[]{:S(2)}) collective-permute-start(bf16[3,256]{1,0:T(4,128)(2,1)} %get-tuple-element.57), channel_id=1, source_target_pairs={{0,4},{4,8},{8,12},{1,5},{5,9},{9,13},{2,6},{6,10},{10,14},{3,7},{... | collective-permute-start | bytes 4616 | tf_op jit(solution)/shard_map/ppermute | solution.py:16
  10.3 0.7 convolution_convert_fusion.3
  11.6 3.5 %collective-permute-start.1 = (bf16[3,256]{1,0:T(4,128)(2,1)}, bf16[3,256]{1,0:T(4,128)(2,1)}, u32[]{:S(2)}, u32[]{:S(2)}) collective-permute-start(bf16[3,256]{1,0:T(4,128)(2,1)} %get-tuple-element.54), channel_id=1, source_target_pairs={{0,4},{4,8},{8,12},{1,5},{5,9},{9,13},{2,6},{6,10},{10,14},{3,7},{... | collective-permute-start | bytes 4616 | tf_op jit(solution)/shard_map/ppermute | solution.py:16
  15.2 0.9 multiply_exponential_fusion
  16.1 1.4 %multiply_subtract_fusion = (f32[512,8]{0,1:T(8,128)S(1)}, f32[512,8]{0,1:T(8,128)S(1)}) fusion(f32[512,8]{0,1:T(8,128)S(1)} %copy-done.8, f32[8]{0:T(128)S(1)} %get-tuple-element.29, f32[8]{0:T(128)S(1)} %dynamic_slice.37, bf16[512,2048]{1,0:T(8,128)(2,1)S(1)} %copy-done, bf16[2048,32]{0,1:T(8,128)(2,1)} %param.21, s32[]{:T(128)S(6)} %select_n.61), kind=kOutput, calls=%fused_computation.98 | convolution fusion | flops 16814080 | bytes 2179140 | tf_op jit(solution)/shard_map/dot_general | solution.py:94
  18.7 3.2 %all-to-all-start.1 = ((f32[4,1,2,4]{3,2,1,0:T(2,128)}), f32[4,1,2,4]{3,2,1,0:T(2,128)S(1)}, u32[]{:S(2)}, u32[]{:S(2)}) async-start(f32[4,1,2,4]{3,2,1,0:T(2,128)} %stack.4), calls=%async_computation.1 | async-start | bytes 8192 | tf_op jit(solution)/shard_map/all_to_all | solution.py:133
  21.9 2.8 %convolution_convert_fusion.1 = bf16[512,512]{1,0:T(8,128)(2,1)S(1)} fusion(bf16[512,2048]{1,0:T(8,128)(2,1)S(1)} %copy-done, bf16[2048,512]{1,0:T(8,128)(2,1)} %param.17), kind=kOutput, calls=%fused_computation.9 | convolution fusion | flops 1074003968 | bytes 4718592 | tf_op jit(solution)/shard_map/dot_general | solution.py:25
  24.8 0.8 copy-done.6
  26.2 3.9 %collective-permute-start = (bf16[3,512]{1,0:T(4,128)(2,1)}, bf16[3,512]{1,0:T(4,128)(2,1)S(1)}, u32[]{:S(2)}, u32[]{:S(2)}) collective-permute-start(bf16[3,512]{1,0:T(4,128)(2,1)} %get-tuple-element.52), channel_id=1, source_target_pairs={{0,4},{4,8},{8,12},{1,5},{5,9},{9,13},{2,6},{6,10},{10,14},{3,7},{... | collective-permute-start | bytes 9224 | tf_op jit(solution)/shard_map/ppermute | solution.py:16
  30.6 1.6 %fusion.99 = f32[1,256]{1,0:T(1,128)S(1)} fusion(bf16[2048,1]{0,1:T(2,128)(2,1)S(1)} %reshape.253, bf16[2048,256]{1,0:T(8,128)(2,1)} %param.18), kind=kOutput, calls=%fused_computation.198 | convolution fusion | flops 1048576 | bytes 1053696 | tf_op jit(solution)/shard_map/dot_general | solution.py:25
  32.2 1.5 %fusion.98 = f32[1,256]{1,0:T(1,128)S(1)} fusion(bf16[2048,1]{0,1:T(2,128)(2,1)S(1)} %reshape.253, bf16[2048,256]{1,0:T(8,128)(2,1)} %param.19), kind=kOutput, calls=%fused_computation.197 | convolution fusion | flops 1048576 | bytes 1053696 | tf_op jit(solution)/shard_map/dot_general | solution.py:25
  34.8 0.7 mul.552
  35.5 0.7 mul.510
  37.3 0.7 mul.529
  37.9 0.6 mul.533
  38.6 2.5 %fusion.101 = f32[1,512]{1,0:T(1,128)} fusion(bf16[2048,1]{0,1:T(2,128)(2,1)S(1)} %reshape.253, bf16[2048,512]{1,0:T(8,128)(2,1)} %param.20), kind=kOutput, calls=%fused_computation.200 | convolution fusion | flops 2097152 | bytes 2103296 | tf_op jit(solution)/shard_map/dot_general | solution.py:25
  41.6 10.0 %all-reduce = (bf16[3,512]{1,0:T(4,128)(2,1)S(1)}, bf16[3,256]{1,0:T(4,128)(2,1)S(1)}, bf16[3,256]{1,0:T(4,128)(2,1)S(1)}) all-reduce(bf16[3,512]{1,0:T(4,128)(2,1)S(1)} %get-tuple-element.53, bf16[3,256]{1,0:T(4,128)(2,1)S(1)} %get-tuple-element.56, ...), channel_id=1, replica_groups=mesh['grp'=2,'sp'=4,'tp'=4] {'sp'}, use_global_device_ids=true, to_apply=%region_7.8 | all-reduce | flops 3072 | bytes 12288 | tf_op jit(solution)/shard_map/psum | solution.py:21
  51.7 0.7 reshape.247
  52.4 0.7 maximum_convert_fusion.4
  53.1 1.5 %convert_reduce_fusion.1 = (bf16[256]{0:T(256)(128)(2,1)S(1)}, f32[1,256]{1,0:T(1,128)}, f32[1,256]{1,0:T(1,128)}, f32[1,256]{1,0:T(1,128)}, f32[1,256]{1,0:T(1,128)}) fusion(f32[4,256]{1,0:T(4,128)S(1)} %get-tuple-element.63, bf16[4,1024]{1,0:T(4,128)(2,1)} %param.24, s32[]{:T(128)S(6)} %select_n.60, s32[]{:T(128)S(6)} %add.243, s32[]{:T(128)S(6)} %add.244, ...), kind=kLoop, calls=%fused_computation.182 | loop fusion | flops 4096 | bytes 10768 | tf_op jit(solution)/shard_map/convert_element_type | solution.py:191
  54.6 1.5 %convert_convert_fusion = (f32[1,256]{1,0:T(1,128)S(1)}, f32[1,256]{1,0:T(1,128)}, f32[1,256]{1,0:T(1,128)}, f32[1,256]{1,0:T(1,128)}, f32[1,256]{1,0:T(1,128)}) fusion(f32[4,256]{1,0:T(4,128)S(1)} %get-tuple-element.64, bf16[4,1024]{1,0:T(4,128)(2,1)} %param.23, s32[]{:T(128)S(6)} %select_n.60, s32[]{:T(128)S(6)} %add.243, s32[]{:T(128)S(6)} %add.244, ...), kind=kLoop, calls=%fused_computation.181 | loop fusion | flops 4352 | bytes 11280 | tf_op jit(solution)/shard_map/reshape | solution.py:193
  56.8 1.5 %fusion.93 = (f32[4,128,2,4]{3,2,1,0:T(2,128)}, f32[4,128,2,4]{3,2,1,0:T(2,128)}) fusion(f32[4,128,2,4]{3,2,1,0:T(2,128)S(1)} %fusion.97, f32[4,128,2,4]{3,2,1,0:T(2,128)S(1)} %copy.152, f32[4,2,4]{2,1,0:T(2,128)S(1)} %get-tuple-element.47), kind=kLoop, calls=%fused_computation.191 | loop fusion | flops 8192 | bytes 65664 | tf_op jit(solution)/shard_map/exp | solution.py:166
  58.4 1.2 copy.151
  59.6 1.3 copy.153
  60.9 1.3 broadcast_multiply_fusion
  62.8 0.7 copy.160
  63.5 0.7 copy.159
  64.2 0.7 copy.177
  64.8 1.0 maximum_convert_fusion.2
  65.9 1.0 multiply_convert_fusion.5
  66.9 0.7 maximum_convert_fusion.1
  68.1 1.2 maximum_convert_fusion
  69.3 0.6 multiply_convert_fusion.4
  70.0 1.0 copy.143
  71.0 2.0 %reshape.234 = bf16[4,128,2,4,64]{1,0,4,3,2:T(4,128)(2,1)} reshape(bf16[512,512]{0,1:T(8,128)(2,1)} %copy.143) | data formatting | bytes 1048576 | tf_op jit(solution)/shard_map/reshape | solution.py:109
  73.0 1.2 multiply_convert_fusion.3
  74.5 1.0 slice_add_fusion
  75.8 1.2 reshape.276
  76.9 3.6 %all-to-all-start = ((f32[4,1,16384]{2,1,0:T(1,128)}), f32[4,1,16384]{2,1,0:T(1,128)S(1)}, u32[]{:S(2)}, u32[]{:S(2)}) async-start(f32[4,1,16384]{2,1,0:T(1,128)} %reshape.276), calls=%async_computation | async-start | bytes 524288 | tf_op jit(solution)/shard_map/all_to_all | solution.py:138
  80.8 2.9 %convolution_bitcast_fusion.2 = f32[4,128,2,4,64]{1,4,3,2,0:T(8,128)} fusion(f32[4,2,4,128]{3,2,1,0:T(4,128)S(1)} %copy.149, f32[4,2,4,128]{3,2,1,0:T(4,128)S(1)} %copy.147, f32[4,2,128,128]{3,2,1,0:T(8,128)S(1)} %fusion.40, pred[128,128]{1,0:T(8,128)(4,1)S(1)} %iota_compare_fusion, bf16[4,128,2,4,64]{1,0,4,3,2:T(4,128)(2,1)} %reshape.234), kind=kOutput, calls=%fused_computation.5 | convolution fusion | flops 69730304 | bytes 2146304 | tf_op jit(solution)/shard_map/bgels,bsgep->blgep/dot_general | solution.py:162
  83.8 3.3 %all-to-all-done = f32[4,1,16384]{2,1,0:T(1,128)S(1)} async-done(((f32[4,1,16384]{2,1,0:T(1,128)}), f32[4,1,16384]{2,1,0:T(1,128)S(1)}, u32[]{:S(2)}, u32[]{:S(2)}) %all-to-all-start) | async-done | bytes 262176 | tf_op jit(solution)/shard_map/all_to_all | solution.py:138
  87.7 1.4 %reduce.9 = f32[4,16384]{1,0:T(4,128)S(1)} reduce(f32[4,1,16384]{2,1,0:T(1,128)S(1)} %all-to-all-done, f32[]{:T(128)} %broadcast.119), dimensions={1}, to_apply=%all_to_all.8.reduce_sub_computation | reduce | bytes 524292 | tf_op jit(solution)/shard_map/all_to_all | solution.py:138
  89.4 2.0 %fusion.35 = bf16[2,4,1,32,64]{4,2,3,1,0:T(2,128)(2,1)S(1)} fusion(f32[4,2,4,1,1]{0,3,4,2,1:T(1,128)} %copy.177, f32[4,32,2,4,64]{4,3,2,1,0:T(4,128)S(1)} %bitcast.132), kind=kOutput, calls=%fused_computation.69 | convolution fusion | flops 786432 | bytes 295040 | tf_op jit(solution)/shard_map/kge,kngep->ngep/dot_general | solution.py:146
  91.4 2.0 %convolution_bitcast_fusion.3 = f32[4,32,2,4,64]{4,0,1,3,2:T(4,128)S(1)} fusion(f32[4,32,2,4,64]{4,3,2,1,0:T(4,128)S(1)} %bitcast.133, f32[4,2,4]{0,2,1:T(4,128)} %copy.160, f32[4,2,4]{0,2,1:T(4,128)} %copy.159, pred[4,4]{1,0:T(4,128)(4,1)} %iota_compare_fusion.1), kind=kOutput, calls=%fused_computation.10 | convolution fusion | flops 3145984 | bytes 524560 | tf_op jit(solution)/shard_map/jkge,kngep->jngep/dot_general | solution.py:142
  93.5 1.0 reshape.278
  94.6 3.4 %all-to-all-start.2 = ((f32[4,1,16384]{2,1,0:T(1,128)}), f32[4,1,16384]{2,1,0:T(1,128)S(1)}, u32[]{:S(2)}, u32[]{:S(2)}) async-start(f32[4,1,16384]{2,1,0:T(1,128)} %reshape.278), calls=%async_computation.2 | async-start | bytes 524288 | tf_op jit(solution)/shard_map/all_to_all | solution.py:149
  98.0 0.9 bitcast_add_fusion
  98.9 0.8 fusion.43
  99.7 12.2 %psum.31 = f32[2,4,64]{2,1,0:T(4,128)S(1)} all-reduce(f32[2,4,64]{2,1,0:T(4,128)S(1)} %bitcast.146), channel_id=1, replica_groups=mesh['grp'=2,'sp'=4,'tp'=4] {'sp'}, use_global_device_ids=true, to_apply=%region_8.9 | all-reduce | flops 512 | bytes 4096 | tf_op jit(solution)/shard_map/psum | solution.py:202
  111.9 0.7 multiply_add_fusion
  112.7 0.7 fusion.90
  113.6 0.7 convert_element_type.211
  114.4 0.8 multiply_convert_fusion.7
  116.0 1.4 %reduce.10 = f32[4,16384]{1,0:T(4,128)S(1)} reduce(f32[4,1,16384]{2,1,0:T(1,128)S(1)} %all-to-all-done.2, f32[]{:T(128)} %broadcast.119), dimensions={1}, to_apply=%all_to_all.22.reduce_sub_computation | reduce | bytes 524292 | tf_op jit(solution)/shard_map/all_to_all | solution.py:149
  117.7 0.9 copy.164
  118.6 2.3 %fusion.1 = f32[4,128,2,4,64]{1,4,3,2,0:T(8,128)S(1)} fusion(f32[4,128,2,4,64]{1,4,3,2,0:T(8,128)} %convolution_bitcast_fusion.2, f32[1,128,2,4,64]{1,4,3,2,0:T(8,128)} %get-tuple-element.41, f32[1,128,2,4,64]{1,4,3,2,0:T(8,128)} %get-tuple-element.42, f32[1,128,2,4,64]{1,4,3,2,0:T(8,128)} %get-tuple-element.43, f32[4]{0:T(128)} %pad.6.clone, ...), kind=kOutput, calls=%fused_computation.4 | convolution fusion | flops 404488192 | bytes 3424400 | tf_op jit(solution)/shard_map/blgn,bngep->blgep/dot_general | solution.py:166
  120.9 1.8 %copy.188 = f32[4,128,2,4,64]{4,3,2,1,0:T(4,128)} copy(f32[4,128,2,4,64]{1,4,3,2,0:T(8,128)S(1)} %fusion.1) | data formatting | bytes 2097152 | tf_op jit(solution)/shard_map/reshape | solution.py:172
  122.8 3.5 %reshape.265 = f32[512,512]{1,0:T(8,128)} reshape(f32[4,128,2,4,64]{4,3,2,1,0:T(4,128)} %copy.188) | data formatting | bytes 2097152 | tf_op jit(solution)/shard_map/reshape | solution.py:172
  126.3 4.6 %fusion.96 = (f32[512,512]{1,0:T(8,128)}, f32[512,512]{1,0:T(8,128)}) fusion(bf16[512,2048]{1,0:T(8,128)(2,1)S(1)} %copy-done, bf16[2048,512]{1,0:T(8,128)(2,1)} %param.20, f32[512,512]{1,0:T(8,128)} %reshape.265, bf16[512,512]{1,0:T(8,128)(2,1)S(1)} %copy-done.2, f32[512]{0:T(512)S(1)} %copy-done.15), kind=kOutput, calls=%fused_computation.194 | convolution fusion | flops 1076625408 | bytes 7866368 | tf_op jit(solution)/shard_map/dot_general | solution.py:25
  130.9 1.9 %mul.516 = f32[512,2,256]{2,1,0:T(2,128)S(1)} reshape(f32[512,512]{1,0:T(8,128)} %get-tuple-element.61) | data formatting | bytes 2097152 | tf_op jit(solution)/shard_map/mul | solution.py:39
  132.8 0.6 reduce_sum.28
  134.6 1.1 multiply_convert_fusion.2
  (101 shorter events, 12.9 us)
Async XLA Ops:
  0.6 1.6 %copy-start = (bf16[512,2048]{1,0:T(8,128)(2,1)S(1)}, bf16[512,2048]{1,0:T(8,128)(2,1)}, u32[]{:S(2)}) copy-start(bf16[512,2048]{1,0:T(8,128)(2,1)} %param.15) | copy-start | bytes 6291460
  0.6 9.7 %copy-start.4 = (bf16[2048,256]{1,0:T(8,128)(2,1)S(1)}, bf16[2048,256]{1,0:T(8,128)(2,1)}, u32[]{:S(2)}) copy-start(bf16[2048,256]{1,0:T(8,128)(2,1)} %param.19) | copy-start | bytes 3145732
  4.2 6.9 %copy-start.7 = (bf16[512,256]{1,0:T(8,128)(2,1)}, bf16[512,256]{1,0:T(8,128)(2,1)S(1)}, u32[]{:S(2)}) copy-start(bf16[512,256]{1,0:T(8,128)(2,1)S(1)} %convolution_convert_fusion.2) | copy-start | bytes 786436
  4.2 10.9 %copy-start.14 = (bf16[2048]{0:T(1024)(128)(2,1)S(1)}, bf16[2048]{0:T(1024)(128)(2,1)}, u32[]{:S(2)}) copy-start(bf16[2048]{0:T(1024)(128)(2,1)} %param.16) | copy-start | bytes 12292
  4.2 10.9 %copy-start.17 = (f32[32]{0:T(128)S(1)}, f32[32]{0:T(128)}, u32[]{:S(2)}) copy-start(f32[32]{0:T(128)} %param.26) | copy-start | bytes 388
  4.2 11.0 %copy-start.16 = (f32[32]{0:T(128)S(1)}, f32[32]{0:T(128)}, u32[]{:S(2)}) copy-start(f32[32]{0:T(128)} %param.25) | copy-start | bytes 388
  4.2 11.9 %copy-start.8 = (f32[512,8]{0,1:T(8,128)S(1)}, f32[512,8]{0,1:T(8,128)}, u32[]{:S(2)}) copy-start(f32[512,8]{0,1:T(8,128)} %param.27) | copy-start | bytes 49156
  4.8 60.0 %collective-permute-start.2 = (bf16[3,256]{1,0:T(4,128)(2,1)}, bf16[3,256]{1,0:T(4,128)(2,1)}, u32[]{:S(2)}, u32[]{:S(2)}) collective-permute-start(bf16[3,256]{1,0:T(4,128)(2,1)} %get-tuple-element.57), channel_id=1, source_target_pairs={{0,4},{4,8},{8,12},{1,5},{5,9},{9,13},{2,6},{6,10},{10,14},{3,7},{... | collective-permute-start | bytes 4616 | tf_op jit(solution)/shard_map/ppermute | solution.py:16
  11.6 55.3 %collective-permute-start.1 = (bf16[3,256]{1,0:T(4,128)(2,1)}, bf16[3,256]{1,0:T(4,128)(2,1)}, u32[]{:S(2)}, u32[]{:S(2)}) collective-permute-start(bf16[3,256]{1,0:T(4,128)(2,1)} %get-tuple-element.54), channel_id=1, source_target_pairs={{0,4},{4,8},{8,12},{1,5},{5,9},{9,13},{2,6},{6,10},{10,14},{3,7},{... | collective-permute-start | bytes 4616 | tf_op jit(solution)/shard_map/ppermute | solution.py:16
  18.7 44.1 %all-to-all-start.1 = ((f32[4,1,2,4]{3,2,1,0:T(2,128)}), f32[4,1,2,4]{3,2,1,0:T(2,128)S(1)}, u32[]{:S(2)}, u32[]{:S(2)}) async-start(f32[4,1,2,4]{3,2,1,0:T(2,128)} %stack.4), calls=%async_computation.1 | async-start | bytes 8192 | tf_op jit(solution)/shard_map/all_to_all | solution.py:133
  24.8 0.8 copy-start.6
  26.2 42.0 %collective-permute-start = (bf16[3,512]{1,0:T(4,128)(2,1)}, bf16[3,512]{1,0:T(4,128)(2,1)S(1)}, u32[]{:S(2)}, u32[]{:S(2)}) collective-permute-start(bf16[3,512]{1,0:T(4,128)(2,1)} %get-tuple-element.52), channel_id=1, source_target_pairs={{0,4},{4,8},{8,12},{1,5},{5,9},{9,13},{2,6},{6,10},{10,14},{3,7},{... | collective-permute-start | bytes 9224 | tf_op jit(solution)/shard_map/ppermute | solution.py:16
  30.1 3.6 %copy-start.3 = (bf16[2048,512]{1,0:T(8,128)(2,1)S(1)}, bf16[2048,512]{1,0:T(8,128)(2,1)}, u32[]{:S(2)}) copy-start(bf16[2048,512]{1,0:T(8,128)(2,1)} %param.17) | copy-start | bytes 6291460
  30.6 4.1 %copy-start.18 = (f32[32]{0:T(128)S(1)}, f32[32]{0:T(128)}, u32[]{:S(2)}) copy-start(f32[32]{0:T(128)} %param.28) | copy-start | bytes 388
  34.0 17.6 %copy-start.13 = (bf16[4,2048]{1,0:T(4,128)(2,1)S(1)}, bf16[4,2048]{1,0:T(4,128)(2,1)}, u32[]{:S(2)}) copy-start(bf16[4,2048]{1,0:T(4,128)(2,1)} %param.22) | copy-start | bytes 49156
  60.8 6.8 %copy-start.9 = (f32[1,256]{1,0:T(1,128)S(1)}, f32[1,256]{1,0:T(1,128)}, u32[]{:S(2)}) copy-start(f32[1,256]{1,0:T(1,128)} %get-tuple-element.24) | copy-start | bytes 3076
  60.8 6.8 %copy-start.10 = (f32[1,256]{1,0:T(1,128)S(1)}, f32[1,256]{1,0:T(1,128)}, u32[]{:S(2)}) copy-start(f32[1,256]{1,0:T(1,128)} %get-tuple-element.25) | copy-start | bytes 3076
  60.8 6.8 %copy-start.11 = (f32[1,256]{1,0:T(1,128)S(1)}, f32[1,256]{1,0:T(1,128)}, u32[]{:S(2)}) copy-start(f32[1,256]{1,0:T(1,128)} %get-tuple-element.26) | copy-start | bytes 3076
  60.8 6.8 %copy-start.12 = (f32[1,256]{1,0:T(1,128)S(1)}, f32[1,256]{1,0:T(1,128)}, u32[]{:S(2)}) copy-start(f32[1,256]{1,0:T(1,128)} %get-tuple-element.27) | copy-start | bytes 3076
  70.0 4.5 %copy-start.1 = (bf16[512,512]{1,0:T(8,128)(2,1)}, bf16[512,512]{1,0:T(8,128)(2,1)S(1)}, u32[]{:S(2)}) copy-start(bf16[512,512]{1,0:T(8,128)(2,1)S(1)} %multiply_convert_fusion.4) | copy-start | bytes 1572868
  76.9 10.2 %all-to-all-start = ((f32[4,1,16384]{2,1,0:T(1,128)}), f32[4,1,16384]{2,1,0:T(1,128)S(1)}, u32[]{:S(2)}, u32[]{:S(2)}) async-start(f32[4,1,16384]{2,1,0:T(1,128)} %reshape.276), calls=%async_computation | async-start | bytes 524288 | tf_op jit(solution)/shard_map/all_to_all | solution.py:138
  94.6 21.4 %all-to-all-start.2 = ((f32[4,1,16384]{2,1,0:T(1,128)}), f32[4,1,16384]{2,1,0:T(1,128)S(1)}, u32[]{:S(2)}, u32[]{:S(2)}) async-start(f32[4,1,16384]{2,1,0:T(1,128)} %reshape.278), calls=%async_computation.2 | async-start | bytes 524288 | tf_op jit(solution)/shard_map/all_to_all | solution.py:149
  122.7 3.5 %copy-start.2 = (bf16[512,512]{1,0:T(8,128)(2,1)S(1)}, bf16[512,512]{1,0:T(8,128)(2,1)}, u32[]{:S(2)}) copy-start(bf16[512,512]{1,0:T(8,128)(2,1)} %copy-done.1) | copy-start | bytes 1572868
  122.8 3.5 %copy-start.15 = (f32[512]{0:T(512)S(1)}, f32[512]{0:T(512)}, u32[]{:S(2)}) copy-start(f32[512]{0:T(512)} %mul.510) | copy-start | bytes 6148
  133.4 1.2 copy-start.5
